TPU v7x, 32 devices: a whole 2x2x4 slice. The times are simulated.
32 devices in a mesh: ep: 8 (over z, x), tp: 4 (over y, core).
Axes of the slice: x: 2, y: 2, z: 4, core: 2. Of those that a mesh axis runs over, the one named last changes fastest.
Arguments:
- tokens: bfloat16 [192, 4096], P('ep'), may hold values from -6 to 6
- delta_state: float32 [192, 16, 128, 128], P('ep', 'tp'), may hold values from -0.625 to 0.625
- attn_gain: float32 [4096], replicated, may hold values from 0.1 to 1.9
- query_weight: bfloat16 [4096, 2048], P('ep', 'tp'), may hold values from -0.09375 to 0.09375
- key_weight: bfloat16 [4096, 2048], P('ep', 'tp'), may hold values from -0.09375 to 0.09375
- value_weight: bfloat16 [4096, 2048], P('ep', 'tp'), may hold values from -0.09375 to 0.09375
- decay_weight: bfloat16 [4096, 16], replicated, may hold values from -0.09375 to 0.09375
- beta_weight: bfloat16 [4096, 16], replicated, may hold values from -0.09375 to 0.09375
- decay_rate: float32 [16], P('tp'), may hold values from 0.05 to 3
- head_gain: float32 [128], replicated, may hold values from 0.1 to 1.9
- output_weight: bfloat16 [2048, 4096], P('tp'), may hold values from -0.125 to 0.125
- ffn_gain: float32 [4096], replicated, may hold values from 0.1 to 1.9
- expert_ids: int32 [192, 2], P('ep'), may hold values from 0 to 7, all different within a row; in each aligned block of 24 rows (0 to 23, 24 to 47, ...) at most 12 rows name the same one
- group_prob: float32 [192], P('ep'), may hold values from 0.3 to 1
- expert_logit: float32 [192, 2], P('ep'), may hold values from -8 to 8
- expert_gate: bfloat16 [8, 4096, 1024], P('ep', None, 'tp'), may hold values from -0.09375 to 0.09375
- expert_up: bfloat16 [8, 4096, 1024], P('ep', None, 'tp'), may hold values from -0.09375 to 0.09375
- expert_down: bfloat16 [8, 1024, 4096], P('ep', 'tp'), may hold values from -0.1875 to 0.1875
- dense_gate: bfloat16 [4096, 4096], P('tp', 'ep'), may hold values from -0.09375 to 0.09375
- dense_up: bfloat16 [4096, 4096], P('tp', 'ep'), may hold values from -0.09375 to 0.09375
- dense_down: bfloat16 [4096, 4096], P('ep', 'tp'), may hold values from -0.09375 to 0.09375
- dense_mix: float32 [4096], P('tp'), may hold values from -3 to 3
Outputs:
- mixed_out: bfloat16 [192, 4096], P('ep', 'tp')
- new_state: float32 [192, 16, 128, 128], P('ep', 'tp')
Inputs may be any that keep to these rules, and one draw needn't show every extreme that they name: `expert_ids`: each row names 2 different experts. Among the rows of one device (aligned blocks of 24 rows) no expert is named by more than 12 rows, and in every draw some expert reaches 12 in some block.
All inputs are finite; a program needn't handle non-finite values.
Results may differ from a plain program's by a relative error of at most 0.02.
Values may be sent and summed in bfloat16 or wider, within the bound.
A program may use at most 64 MiB of HBM per device.

v0:
```python
import jax
import jax.numpy as jnp
from jax import lax
from jax.sharding import PartitionSpec as P

EPS = 1e-06


def rms_scale(values, gain):
    mean_sq = jnp.mean(values * values, axis=-1, keepdims=True)
    return values * lax.rsqrt(mean_sq + EPS) * gain


def unit_rows(values):
    return values * lax.rsqrt(jnp.sum(values * values, axis=-1, keepdims=True) + EPS)


def per_device(
    tokens,
    delta_state,
    attn_gain,
    query_weight,
    key_weight,
    value_weight,
    decay_weight,
    beta_weight,
    decay_rate,
    head_gain,
    output_weight,
    ffn_gain,
    expert_ids,
    group_prob,
    expert_logit,
    expert_gate,
    expert_up,
    expert_down,
    dense_gate,
    dense_up,
    dense_down,
    dense_mix,
):
    seq_rows = tokens.shape[0]
    head_count = delta_state.shape[1]
    head_size = delta_state.shape[2]
    width_local = head_count * head_size
    tp_index = lax.axis_index("tp")
    residual = tokens.astype(jnp.float32)
    normed = rms_scale(residual, attn_gain).astype(jnp.bfloat16)
    spread = lax.all_to_all(normed, "ep", split_axis=1, concat_axis=0, tiled=True)
    joined = jnp.concatenate((query_weight, key_weight, value_weight), axis=1)
    summed = lax.psum_scatter(
        jnp.dot(spread, joined, preferred_element_type=jnp.float32).astype(jnp.bfloat16),
        "ep",
        scatter_dimension=0,
        tiled=True,
    ).astype(jnp.float32)
    query_sum = summed[:, :width_local]
    key_sum = summed[:, width_local : 2 * width_local]
    value_sum = summed[:, 2 * width_local :]

    def heads_of(values):
        rounded = lax.optimization_barrier(values.astype(jnp.bfloat16))
        return rounded.astype(jnp.float32).reshape(seq_rows, head_count, head_size)

    query_unit = unit_rows(heads_of(query_sum)) * head_size ** (-0.5)
    key_unit = unit_rows(heads_of(key_sum))
    value_heads = heads_of(value_sum)
    decay_cols = lax.dynamic_slice_in_dim(decay_weight, tp_index * head_count, head_count, 1)
    beta_cols = lax.dynamic_slice_in_dim(beta_weight, tp_index * head_count, head_count, 1)
    decay_pre = jnp.dot(normed, decay_cols, preferred_element_type=jnp.float32)
    decay = jnp.exp(-decay_rate * jax.nn.softplus(decay_pre))
    beta_gate = jax.nn.sigmoid(jnp.dot(normed, beta_cols, preferred_element_type=jnp.float32))
    recalled = jnp.einsum("bhk,bhkv->bhv", key_unit, delta_state, precision=lax.Precision.HIGHEST)
    correction = beta_gate[..., None] * (value_heads - decay[..., None] * recalled)
    new_state = (
        decay[..., None, None] * delta_state + key_unit[..., :, None] * correction[..., None, :]
    )
    read_out = jnp.einsum("bhk,bhkv->bhv", query_unit, new_state, precision=lax.Precision.HIGHEST)
    head_out = rms_scale(read_out, head_gain).astype(jnp.bfloat16).reshape(seq_rows, width_local)
    attn_part = jnp.dot(head_out, output_weight, preferred_element_type=jnp.float32)
    attn_sum = lax.psum(attn_part.astype(jnp.bfloat16), "tp").astype(jnp.float32)
    middle = residual + attn_sum
    ffn_in = rms_scale(middle, ffn_gain).astype(jnp.bfloat16)
    slice_width = dense_gate.shape[0]
    hidden_width = dense_gate.shape[1]
    own_columns = lax.dynamic_slice_in_dim(ffn_in, tp_index * slice_width, slice_width, 1)
    gate_up = jnp.concatenate((dense_gate, dense_up), axis=1)
    dense_part = jnp.dot(
        lax.all_gather(own_columns, "ep", axis=0, tiled=True),
        gate_up,
        preferred_element_type=jnp.float32,
    )
    dense_sum = lax.psum(dense_part.astype(jnp.bfloat16), "tp").astype(jnp.float32)
    dense_hidden = (jax.nn.silu(dense_sum[:, :hidden_width]) * dense_sum[:, hidden_width:]).astype(
        jnp.bfloat16
    )
    dense_out = lax.psum_scatter(
        jnp.dot(dense_hidden, dense_down, preferred_element_type=jnp.float32).astype(jnp.bfloat16),
        "ep",
        scatter_dimension=0,
        tiled=True,
    ).astype(jnp.float32)
    expert_count = lax.axis_size("ep")
    top_count = expert_ids.shape[1]
    capacity = max(2, 2 * seq_rows * top_count // expert_count)
    pair_ids = expert_ids.reshape(-1)
    onehot = (pair_ids[:, None] == jnp.arange(expert_count, dtype=jnp.int32)[None, :]).astype(
        jnp.int32
    )
    ranks = jnp.sum(onehot * (jnp.cumsum(onehot, axis=0) - 1), axis=1)
    places = pair_ids * capacity + ranks
    dispatch = (
        jnp.arange(expert_count * capacity, dtype=jnp.int32)[:, None] == places[None, :]
    ).astype(jnp.bfloat16)
    repeated = jnp.repeat(ffn_in, top_count, axis=0)
    outgoing = jnp.dot(dispatch, repeated, preferred_element_type=jnp.float32).astype(jnp.bfloat16)
    outgoing = outgoing.reshape(expert_count, capacity, ffn_in.shape[1])
    arrived = lax.all_to_all(outgoing, "ep", split_axis=0, concat_axis=0, tiled=True)
    gate_vals = jnp.einsum(
        "snd,df->snf", arrived, expert_gate[0], preferred_element_type=jnp.float32
    )
    up_vals = jnp.einsum("snd,df->snf", arrived, expert_up[0], preferred_element_type=jnp.float32)
    expert_hidden = (jax.nn.silu(gate_vals) * up_vals).astype(jnp.bfloat16)
    partial_value = jnp.einsum(
        "snf,fd->snd", expert_hidden, expert_down[0], preferred_element_type=jnp.float32
    )
    summed_cols = lax.psum_scatter(
        partial_value.astype(jnp.bfloat16), "tp", scatter_dimension=2, tiled=True
    )
    returned = lax.all_to_all(summed_cols, "ep", split_axis=0, concat_axis=0, tiled=True)
    flat_back = returned.reshape(expert_count * capacity, slice_width)
    picked = (
        jnp.take(flat_back, places, axis=0)
        .astype(jnp.float32)
        .reshape(seq_rows, top_count, slice_width)
    )
    logit_exp = jnp.exp(expert_logit)
    route_weight = group_prob[:, None] * logit_exp / jnp.sum(logit_exp, axis=1, keepdims=True)
    expert_mix = jnp.sum(route_weight[..., None] * picked, axis=1)
    own_middle = lax.dynamic_slice_in_dim(middle, tp_index * slice_width, slice_width, 1)
    mixed_out = (own_middle + jax.nn.sigmoid(dense_mix) * dense_out + expert_mix).astype(
        jnp.bfloat16
    )
    return (mixed_out, new_state)


def solution(mesh):
    return jax.shard_map(
        per_device,
        mesh=mesh,
        in_specs=(
            P("ep", None),
            P("ep", "tp", None, None),
            P(),
            P("ep", "tp"),
            P("ep", "tp"),
            P("ep", "tp"),
            P(),
            P(),
            P("tp"),
            P(),
            P("tp", None),
            P(),
            P("ep", None),
            P("ep"),
            P("ep", None),
            P("ep", None, "tp"),
            P("ep", None, "tp"),
            P("ep", "tp", None),
            P("tp", "ep"),
            P("tp", "ep"),
            P("ep", "tp"),
            P("tp"),
        ),
        out_specs=(P("ep", "tp"), P("ep", "tp", None, None)),
        check_vma=False,
    )
```

profile of v0, /device:TPU:0, one launch (start us, length us, event | category | flops | bytes accessed | tf_op | source)
XLA Modules:
  0.0 333.8 jit_solution(11705922929324244987)
XLA Ops:
  7.2 1.2 fusion.28
  8.4 1.1 fusion.30
  9.6 15.0 %all_to_all.29 = bf16[24,8,512]{2,0,1:T(8,128)(2,1)S(1)} all-to-all(bf16[24,8,512]{2,0,1:T(8,128)(2,1)S(1)} %bitcast.59), channel_id=1, replica_groups=mesh['ep'=8,'tp'=4] {'ep'}, dimensions={1} | all-to-all | bytes 393216 | tf_op jit(solution)/shard_map/all_to_all | solution.py:49
  24.6 2.7 convolution_convert_fusion.3
  27.4 1.0 fusion.48
  28.4 0.1 copy.67
  28.5 1.0 fusion.27
  29.5 0.1 copy.68
  29.6 0.1 copy.73
  29.7 0.1 reshape.151
  30.0 0.2 select_reduce_fusion
  30.1 58.6 %reduce-scatter.4.cloned.1.call-done = bf16[24,1536]{1,0:T(8,128)(2,1)} async-done(((bf16[192,1536]{1,0:T(8,128)(2,1)}), bf16[24,1536]{1,0:T(8,128)(2,1)}) %reduce-scatter.4.cloned.1.call-update) | async-done | bytes 73744 | tf_op jit(solution)/shard_map/reduce_scatter | solution.py:51
  88.8 0.8 fusion.58
  89.6 0.1 multiply_reduce_fusion.3
  89.7 0.1 broadcast_multiply_fusion
  89.8 8.1 %fusion.59 = f32[24,4,1,128]{3,2,1,0:T(1,128)S(1)} fusion(f32[24,4,128,1]{2,3,1,0:T(1,128)S(1)} %bitcast.60, f32[24,4,128,128]{3,2,1,0:T(8,128)} %param.23), kind=kOutput, calls=%fused_computation.93 | convolution fusion | flops 18874368 | bytes 6389760 | tf_op jit(solution)/shard_map/bhk,bhkv->bhv/dot_general | solution.py:73
  97.9 0.1 subtract_multiply_fusion
  98.1 3.9 %multiply_add_fusion = f32[24,4,128,128]{3,2,1,0:T(8,128)} fusion(f32[24,4,128,128]{3,2,1,0:T(8,128)S(1)} %copy-done.1, f32[24,4,128]{2,1,0:T(4,128)S(1)} %subtract_multiply_fusion, f32[24,4,128]{2,1,0:T(4,128)S(1)} %broadcast_multiply_fusion, f32[24,4]{1,0:T(8,128)S(1)} %copy.67), kind=kLoop, calls=%fused_computation.1 | loop fusion | flops 4718592 | bytes 12681600 | tf_op jit(solution)/shard_map/add | solution.py:76
  101.9 0.1 multiply_reduce_fusion.4
  102.1 0.1 multiply_multiply_fusion
  102.2 7.5 %fusion.60 = f32[24,4,1,128]{3,2,1,0:T(1,128)S(1)} fusion(f32[24,4,128,1]{2,3,1,0:T(1,128)S(1)} %bitcast.63, f32[24,4,128,128]{3,2,1,0:T(8,128)} %multiply_add_fusion), kind=kOutput, calls=%fused_computation.94 | convolution fusion | flops 18874368 | bytes 6389760 | tf_op jit(solution)/shard_map/bhk,bhkv->bhv/dot_general | solution.py:78
  109.7 0.1 multiply_reduce_fusion.2
  109.8 0.1 multiply_convert_fusion.1
  109.9 1.4 convolution_convert_fusion.2
  111.3 31.2 %all-reduce.3.cloned.1.call-done = bf16[24,4096]{1,0:T(8,128)(2,1)} async-done(((bf16[24,4096]{1,0:T(8,128)(2,1)}), bf16[24,4096]{1,0:T(8,128)(2,1)}) %all-reduce.3.cloned.1.call-update) | async-done | bytes 196624 | tf_op jit(solution)/shard_map/psum | solution.py:81
  142.5 1.8 convert_add_fusion
  144.3 1.0 multiply_convert_fusion
  145.4 0.3 broadcast_in_dim.10
  145.7 0.2 reshape.152
  145.9 0.3 convolution_convert_fusion.1
  146.2 1.2 reshape.153
  147.4 5.5 %all-to-all-start.1 = ((bf16[8,12,4096]{2,1,0:T(8,128)(2,1)}), bf16[8,12,4096]{2,1,0:T(8,128)(2,1)S(1)}, u32[]{:S(2)}, u32[]{:S(2)}) async-start(bf16[8,12,4096]{2,1,0:T(8,128)(2,1)} %reshape.153), calls=%async_computation.3 | async-start | bytes 2097152 | tf_op jit(solution)/shard_map/all_to_all | solution.py:118
  153.0 45.7 %all_gather.3 = bf16[192,1024]{1,0:T(8,128)(2,1)S(1)} all-gather(bf16[24,1024]{1,0:T(8,128)(2,1)S(1)} %constant_dynamic-slice_fusion), channel_id=1, replica_groups=mesh['ep'=8,'tp'=4] {'ep'}, dimensions={0}, use_global_device_ids=true | all-gather | bytes 442368 | tf_op jit(solution)/shard_map/all_gather | solution.py:89
  198.6 2.9 fusion.14
  201.6 2.0 fusion.7
  203.7 3.9 %convolution_convert_fusion = bf16[8,12,4096]{2,1,0:T(8,128)(2,1)} fusion(bf16[1,256,4096]{2,1,0:T(8,128)(2,1)S(1)} %copy-done, bf16[8,12,4096]{2,1,0:T(8,128)(2,1)S(1)} %all-to-all-done.1, bf16[1,4096,256]{2,1,0:T(8,128)(2,1)} %param.38, f32[8,12,256]{2,1,0:T(8,128)S(1)} %fusion.7), kind=kOutput, calls=%fused_computation.2 | convolution fusion | flops 403193856 | bytes 5865472 | tf_op jit(solution)/shard_map/snf,fd->snd/dot_general | solution.py:124
  207.9 25.3 %all-reduce.5.cloned.1.call-done = bf16[192,1024]{1,0:T(8,128)(2,1)} async-done(((bf16[192,1024]{1,0:T(8,128)(2,1)}), bf16[192,1024]{1,0:T(8,128)(2,1)}) %all-reduce.5.cloned.1.call-update) | async-done | bytes 393232 | tf_op jit(solution)/shard_map/psum | solution.py:93
  233.2 1.1 convert_element_type.71
  234.3 2.4 convolution_convert_fusion.4
  236.8 0.1 mul.260
  236.9 23.5 %reduce-scatter.8.cloned.1.call-done = bf16[8,12,1024]{2,1,0:T(8,128)(2,1)} async-done(((bf16[8,12,4096]{2,1,0:T(8,128)(2,1)}), bf16[8,12,1024]{2,1,0:T(8,128)(2,1)}) %reduce-scatter.8.cloned.1.call-update) | async-done | bytes 196624 | tf_op jit(solution)/shard_map/reduce_scatter | solution.py:127
  260.4 5.5 %all-to-all-start.2 = ((bf16[8,12,1024]{2,1,0:T(8,128)(2,1)}), bf16[8,12,1024]{2,1,0:T(8,128)(2,1)S(1)}, u32[]{:S(2)}, u32[]{:S(2)}) async-start(bf16[8,12,1024]{2,1,0:T(8,128)(2,1)} %reduce-scatter.8.cloned.1.call-done), calls=%async_computation.5 | async-start | bytes 524288 | tf_op jit(solution)/shard_map/all_to_all | solution.py:130
  265.9 0.1 copy.75
  266.1 9.1 %all-to-all-done.2 = bf16[8,12,1024]{2,1,0:T(8,128)(2,1)S(1)} async-done(((bf16[8,12,1024]{2,1,0:T(8,128)(2,1)}), bf16[8,12,1024]{2,1,0:T(8,128)(2,1)S(1)}, u32[]{:S(2)}, u32[]{:S(2)}) %all-to-all-start.2) | async-done | bytes 196640 | tf_op jit(solution)/shard_map/all_to_all | solution.py:130
  275.2 0.7 gather_fusion
  276.0 0.4 multiply_reduce_fusion.1
  276.4 49.3 %reduce-scatter.6.cloned.1.call-done = bf16[24,1024]{1,0:T(8,128)(2,1)} async-done(((bf16[192,1024]{1,0:T(8,128)(2,1)}), bf16[24,1024]{1,0:T(8,128)(2,1)}) %reduce-scatter.6.cloned.1.call-update) | async-done | bytes 49168 | tf_op jit(solution)/shard_map/reduce_scatter | solution.py:97
  325.7 1.6 add_convert_fusion
  (60 shorter events, 1.1 us)
Async XLA Ops:
  7.2 196.5 %copy-start = (bf16[1,256,4096]{2,1,0:T(8,128)(2,1)S(1)}, bf16[1,256,4096]{2,1,0:T(8,128)(2,1)}, u32[]{:S(2)}) copy-start(bf16[1,256,4096]{2,1,0:T(8,128)(2,1)} %param.39) | copy-start | bytes 6291460
  7.2 81.6 %reduce-scatter.4.cloned.1.call-start = ((), (), s32[]{:S(2)}) async-start(), calls=%async_computation.6 | async-start | bytes 663552 | tf_op jit(solution)/shard_map/reduce_scatter | solution.py:51
  9.5 17.8 %copy-start.10 = (f32[4]{0:T(128)S(1)}, f32[4]{0:T(128)}, u32[]{:S(2)}) copy-start(f32[4]{0:T(128)} %param.30) | copy-start | bytes 52
  9.5 20.1 %copy-start.5 = (s32[24,2]{0,1:T(2,128)S(1)}, s32[24,2]{0,1:T(2,128)}, u32[]{:S(2)}) copy-start(s32[24,2]{0,1:T(2,128)} %param.34) | copy-start | bytes 580
  27.3 115.2 %all-reduce.3.cloned.1.call-start = ((), (), s32[]{:S(2)}) async-start(), calls=%async_computation.7 | async-start | bytes 393216 | tf_op jit(solution)/shard_map/psum | solution.py:81
  89.8 8.2 %copy-start.1 = (f32[24,4,128,128]{3,2,1,0:T(8,128)S(1)}, f32[24,4,128,128]{3,2,1,0:T(8,128)}, u32[]{:S(2)}) copy-start(f32[24,4,128,128]{3,2,1,0:T(8,128)} %param.23) | copy-start | bytes 18874372
  102.2 7.6 %copy-start.8 = (f32[128]{0:T(128)S(1)}, f32[128]{0:T(128)}, u32[]{:S(2)}) copy-start(f32[128]{0:T(128)} %param.31) | copy-start | bytes 1540
  102.2 7.7 %copy-start.2 = (bf16[512,4096]{1,0:T(8,128)(2,1)S(1)}, bf16[512,4096]{1,0:T(8,128)(2,1)}, u32[]{:S(2)}) copy-start(bf16[512,4096]{1,0:T(8,128)(2,1)} %param.32) | copy-start | bytes 12582916
  109.7 32.8 %copy-start.3 = (bf16[24,4096]{1,0:T(8,128)(2,1)S(1)}, bf16[24,4096]{1,0:T(8,128)(2,1)}, u32[]{:S(2)}) copy-start(bf16[24,4096]{1,0:T(8,128)(2,1)} %param.22) | copy-start | bytes 589828
  109.7 34.7 %copy-start.4 = (f32[4096]{0:T(1024)S(1)}, f32[4096]{0:T(1024)}, u32[]{:S(2)}) copy-start(f32[4096]{0:T(1024)} %param.33) | copy-start | bytes 49156
  147.4 54.2 %all-to-all-start.1 = ((bf16[8,12,4096]{2,1,0:T(8,128)(2,1)}), bf16[8,12,4096]{2,1,0:T(8,128)(2,1)S(1)}, u32[]{:S(2)}, u32[]{:S(2)}) async-start(bf16[8,12,4096]{2,1,0:T(8,128)(2,1)} %reshape.153), calls=%async_computation.3 | async-start | bytes 2097152 | tf_op jit(solution)/shard_map/all_to_all | solution.py:118
  152.9 80.3 %all-reduce.5.cloned.1.call-start = ((), (), s32[]{:S(2)}) async-start(), calls=%async_computation.8 | async-start | bytes 786432 | tf_op jit(solution)/shard_map/psum | solution.py:93
  201.5 58.9 %reduce-scatter.8.cloned.1.call-start = ((), (), s32[]{:S(2)}) async-start(), calls=%async_computation.10 | async-start | bytes 1310720 | tf_op jit(solution)/shard_map/reduce_scatter | solution.py:127
  203.7 4.2 %copy-start.7 = (f32[24,2]{0,1:T(2,128)S(1)}, f32[24,2]{0,1:T(2,128)}, u32[]{:S(2)}) copy-start(f32[24,2]{0,1:T(2,128)} %param.36) | copy-start | bytes 580
  203.7 4.2 %copy-start.9 = (f32[24]{0:T(128)S(1)}, f32[24]{0:T(128)}, u32[]{:S(2)}) copy-start(f32[24]{0:T(128)} %param.35) | copy-start | bytes 292
  207.6 58.5 %copy-start.6 = (f32[1024]{0:T(1024)S(1)}, f32[1024]{0:T(1024)}, u32[]{:S(2)}) copy-start(f32[1024]{0:T(1024)} %param.43) | copy-start | bytes 12292
  207.6 118.1 %reduce-scatter.6.cloned.1.call-start = ((), (), s32[]{:S(2)}) async-start(), calls=%async_computation.9 | async-start | bytes 442368 | tf_op jit(solution)/shard_map/reduce_scatter | solution.py:97
  260.4 14.8 %all-to-all-start.2 = ((bf16[8,12,1024]{2,1,0:T(8,128)(2,1)}), bf16[8,12,1024]{2,1,0:T(8,128)(2,1)S(1)}, u32[]{:S(2)}, u32[]{:S(2)}) async-start(bf16[8,12,1024]{2,1,0:T(8,128)(2,1)} %reduce-scatter.8.cloned.1.call-done), calls=%async_computation.5 | async-start | bytes 524288 | tf_op jit(solution)/shard_map/all_to_all | solution.py:130
Sparse Core Ops, SparseCore 0:
  27.4 61.3 reduce-scatter.3
  111.4 31.0 all-reduce.2
  201.7 31.4 all-reduce.4
  235.6 24.7 reduce-scatter.7
  263.5 62.1 reduce-scatter.5
where the time goes:
time: 335 us; the launch traced here: 334 us
  waiting for transfers between devices  197 us (59%)
  blocking collectives  60.7 us (18%)
  matrix products  33.2 us (10%)
  between operations  14.1 us (4%)
  other arithmetic  13.2 us (4%)
  starting transfers between devices  11.2 us (3%)
  local copies, waits for them, and re-layouts  4.25 us (1%)
    reduce_scatter x1, waiting for transfers between devices, per_device(): lax.psum_scatter(jnp.dot(spread, joined, preferred_element_type=jnp.float...  58.6 us
    reduce_scatter x1, waiting for transfers between devices, per_device(): lax.psum_scatter(jnp.dot(dense_hidden, dense_down, preferred_element_type...  49.3 us
    all_gather x1, blocking collectives, per_device(): lax.all_gather(own_columns, 'ep', axis=0, tiled=True)  45.7 us
    psum x1, waiting for transfers between devices, per_device(): lax.psum(attn_part.astype(jnp.bfloat16), 'tp').astype(jnp.float32)  31.2 us
    psum x1, waiting for transfers between devices, per_device(): lax.psum(dense_part.astype(jnp.bfloat16), 'tp').astype(jnp.float32)  25.3 us
    reduce_scatter x1, waiting for transfers between devices, per_device(): lax.psum_scatter(partial_value.astype(jnp.bfloat16), 'tp', scatter_dimens...  23.5 us
    all_to_all x1, blocking collectives, per_device(): lax.all_to_all(normed, 'ep', split_axis=1, concat_axis=0, tiled=True)  15 us
    all_to_all x1, waiting for transfers between devices, per_device(): lax.all_to_all(summed_cols, 'ep', split_axis=0, concat_axis=0, tiled=True)  9.06 us
  transfers between devices with their start and end apart: 7, of which 6 were waited for; matrix products, arithmetic and copies ran while one was open for 5% of the time, Pallas kernels for 0%

commit v1 on v0

--- a/solution.py
+++ b/solution.py
@@ -4,6 +4,12 @@
 from jax.sharding import PartitionSpec as P
 
 EPS = 1e-06
+
+
+def add_all(x, mesh_axis):
+    parts = lax.all_gather(x, mesh_axis, axis=0, tiled=False)
+    acc = parts.sum(axis=0)
+    return acc
 
 
 def rms_scale(values, gain):
@@ -78,7 +84,7 @@
     read_out = jnp.einsum("bhk,bhkv->bhv", query_unit, new_state, precision=lax.Precision.HIGHEST)
     head_out = rms_scale(read_out, head_gain).astype(jnp.bfloat16).reshape(seq_rows, width_local)
     attn_part = jnp.dot(head_out, output_weight, preferred_element_type=jnp.float32)
-    attn_sum = lax.psum(attn_part.astype(jnp.bfloat16), "tp").astype(jnp.float32)
+    attn_sum = add_all(attn_part.astype(jnp.bfloat16), "tp").astype(jnp.float32)
     middle = residual + attn_sum
     ffn_in = rms_scale(middle, ffn_gain).astype(jnp.bfloat16)
     slice_width = dense_gate.shape[0]

time: 335 us -> 309 us (0.922)
  waiting for transfers between devices: 197 us -> 166 us
  blocking collectives: 60.7 us -> 70.9 us
    psum x1 -> x0, waiting for transfers between devices: 31.2 us -> none  [per_device(): lax.psum(attn_part.astype(jnp.bfloat16), 'tp').astype(jnp.float32)]
    all_gather x0 -> x1, blocking collectives: none -> 8.59 us  [add_all(): parts = lax.all_gather(x, mesh_axis, axis=0, tiled=False)]
  transfers between devices with their start and end apart: 7 -> 6, of which waited for: 6 -> 5; matrix products, arithmetic and copies ran while one was open for 5% -> 5% of each run, Pallas kernels for 0% -> 0%
where the time goes in v1:
time: 309 us; the launch traced here: 308 us
  waiting for transfers between devices  166 us (54%)
  blocking collectives  70.9 us (23%)
  matrix products  32.5 us (11%)
  between operations  14.2 us (5%)
  other arithmetic  11.5 us (4%)
  starting transfers between devices  9.31 us (3%)
  local copies, waits for them, and re-layouts  4.26 us (1%)
    reduce_scatter x1, waiting for transfers between devices, per_device(): lax.psum_scatter(jnp.dot(spread, joined, preferred_element_type=jnp.float...  58.6 us
    reduce_scatter x1, waiting for transfers between devices, per_device(): lax.psum_scatter(jnp.dot(dense_hidden, dense_down, preferred_element_type...  49.3 us
    all_gather x1, blocking collectives, per_device(): lax.all_gather(own_columns, 'ep', axis=0, tiled=True)  47.3 us
    psum x1, waiting for transfers between devices, per_device(): lax.psum(dense_part.astype(jnp.bfloat16), 'tp').astype(jnp.float32)  24.8 us
    reduce_scatter x1, waiting for transfers between devices, per_device(): lax.psum_scatter(partial_value.astype(jnp.bfloat16), 'tp', scatter_dimens...  23.7 us
    all_to_all x1, blocking collectives, per_device(): lax.all_to_all(normed, 'ep', split_axis=1, concat_axis=0, tiled=True)  15 us
    all_to_all x1, waiting for transfers between devices, per_device(): lax.all_to_all(summed_cols, 'ep', split_axis=0, concat_axis=0, tiled=True)  9.06 us
    all_gather x1, blocking collectives, add_all(): parts = lax.all_gather(x, mesh_axis, axis=0, tiled=False)  8.59 us
  transfers between devices with their start and end apart: 6, of which 5 were waited for; matrix products, arithmetic and copies ran while one was open for 5% of the time, Pallas kernels for 0%

profile of v1, /device:TPU:0, one launch (start us, length us, event | category | flops | bytes accessed | tf_op | source)
XLA Modules:
  0.0 308.2 jit_solution(13727031036999905464)
XLA Ops:
  7.2 1.2 fusion.28
  8.4 1.1 fusion.30
  9.6 15.0 %all_to_all.29 = bf16[24,8,512]{2,0,1:T(8,128)(2,1)S(1)} all-to-all(bf16[24,8,512]{2,0,1:T(8,128)(2,1)S(1)} %bitcast.61), channel_id=1, replica_groups=mesh['ep'=8,'tp'=4] {'ep'}, dimensions={1} | all-to-all | bytes 393216 | tf_op jit(solution)/shard_map/all_to_all | solution.py:55
  24.6 2.7 convolution_convert_fusion.3
  27.3 1.0 fusion.48
  28.4 1.0 fusion.27
  29.4 0.1 copy.68
  29.5 0.1 copy.73
  29.6 0.1 reshape.151
  29.9 0.2 select_reduce_fusion
  30.1 58.6 %reduce-scatter.4.cloned.1.call-done = bf16[24,1536]{1,0:T(8,128)(2,1)} async-done(((bf16[192,1536]{1,0:T(8,128)(2,1)}), bf16[24,1536]{1,0:T(8,128)(2,1)}) %reduce-scatter.4.cloned.1.call-update) | async-done | bytes 73744 | tf_op jit(solution)/shard_map/reduce_scatter | solution.py:57
  88.7 0.8 fusion.58
  89.5 0.1 multiply_reduce_fusion.3
  89.7 0.1 broadcast_multiply_fusion
  89.8 8.1 %fusion.59 = f32[24,4,1,128]{3,2,1,0:T(1,128)S(1)} fusion(f32[24,4,128,1]{2,3,1,0:T(1,128)S(1)} %bitcast.62, f32[24,4,128,128]{3,2,1,0:T(8,128)} %param.23), kind=kOutput, calls=%fused_computation.93 | convolution fusion | flops 18874368 | bytes 6389760 | tf_op jit(solution)/shard_map/bhk,bhkv->bhv/dot_general | solution.py:79
  97.9 0.1 subtract_multiply_fusion
  98.0 3.9 %multiply_add_fusion = f32[24,4,128,128]{3,2,1,0:T(8,128)} fusion(f32[24,4,128,128]{3,2,1,0:T(8,128)S(1)} %copy-done.1, f32[24,4,128]{2,1,0:T(4,128)S(1)} %subtract_multiply_fusion, f32[24,4,128]{2,1,0:T(4,128)S(1)} %broadcast_multiply_fusion, f32[24,4]{1,0:T(8,128)S(1)} %copy.67), kind=kLoop, calls=%fused_computation.1 | loop fusion | flops 4718592 | bytes 12681600 | tf_op jit(solution)/shard_map/add | solution.py:82
  101.9 0.1 multiply_reduce_fusion.4
  102.0 0.1 multiply_multiply_fusion
  102.2 7.5 %fusion.60 = f32[24,4,1,128]{3,2,1,0:T(1,128)S(1)} fusion(f32[24,4,128,1]{2,3,1,0:T(1,128)S(1)} %bitcast.65, f32[24,4,128,128]{3,2,1,0:T(8,128)} %multiply_add_fusion), kind=kOutput, calls=%fused_computation.94 | convolution fusion | flops 18874368 | bytes 6389760 | tf_op jit(solution)/shard_map/bhk,bhkv->bhv/dot_general | solution.py:84
  109.6 0.1 multiply_reduce_fusion.2
  109.8 0.1 multiply_convert_fusion.1
  109.9 0.7 convolution_convert_fusion.2
  110.6 8.6 %all-gather = bf16[96,4096]{1,0:T(8,128)(2,1)S(1)} all-gather(bf16[24,4096]{1,0:T(8,128)(2,1)S(1)} %convolution_convert_fusion.2), channel_id=2, replica_groups=mesh['ep'=8,'tp'=4] {'tp'}, dimensions={0}, use_global_device_ids=true | all-gather | bytes 983040 | tf_op jit(solution)/shard_map/all_gather | solution.py:10
  119.2 0.2 reduce_sum.92
  119.3 0.9 convert_add_fusion
  120.3 0.1 multiply_convert_fusion
  120.4 0.3 broadcast_in_dim.10
  120.7 0.2 reshape.152
  120.9 0.3 convolution_convert_fusion.1
  121.2 1.2 reshape.153
  122.4 3.6 %all-to-all-start.1 = ((bf16[8,12,4096]{2,1,0:T(8,128)(2,1)}), bf16[8,12,4096]{2,1,0:T(8,128)(2,1)S(1)}, u32[]{:S(2)}, u32[]{:S(2)}) async-start(bf16[8,12,4096]{2,1,0:T(8,128)(2,1)} %reshape.153), calls=%async_computation.3 | async-start | bytes 2097152 | tf_op jit(solution)/shard_map/all_to_all | solution.py:124
  126.1 47.3 %all_gather.11 = bf16[192,1024]{1,0:T(8,128)(2,1)S(1)} all-gather(bf16[24,1024]{1,0:T(8,128)(2,1)S(1)} %constant_dynamic-slice_fusion), channel_id=1, replica_groups=mesh['ep'=8,'tp'=4] {'ep'}, dimensions={0}, use_global_device_ids=true | all-gather | bytes 442368 | tf_op jit(solution)/shard_map/all_gather | solution.py:95
  173.4 2.9 fusion.14
  176.4 2.0 fusion.7
  178.4 3.9 %convolution_convert_fusion = bf16[8,12,4096]{2,1,0:T(8,128)(2,1)} fusion(bf16[1,256,4096]{2,1,0:T(8,128)(2,1)S(1)} %copy-done, bf16[8,12,4096]{2,1,0:T(8,128)(2,1)S(1)} %all-to-all-done.1, bf16[1,4096,256]{2,1,0:T(8,128)(2,1)} %param.38, f32[8,12,256]{2,1,0:T(8,128)S(1)} %fusion.7), kind=kOutput, calls=%fused_computation.2 | convolution fusion | flops 403193856 | bytes 5865472 | tf_op jit(solution)/shard_map/snf,fd->snd/dot_general | solution.py:130
  182.7 24.8 %all-reduce.2.cloned.1.call-done = bf16[192,1024]{1,0:T(8,128)(2,1)} async-done(((bf16[192,1024]{1,0:T(8,128)(2,1)}), bf16[192,1024]{1,0:T(8,128)(2,1)}) %all-reduce.2.cloned.1.call-update) | async-done | bytes 393232 | tf_op jit(solution)/shard_map/psum | solution.py:99
  207.5 1.1 convert_element_type.73
  208.6 2.4 convolution_convert_fusion.4
  211.1 0.1 mul.260
  211.2 23.7 %reduce-scatter.8.cloned.1.call-done = bf16[8,12,1024]{2,1,0:T(8,128)(2,1)} async-done(((bf16[8,12,4096]{2,1,0:T(8,128)(2,1)}), bf16[8,12,1024]{2,1,0:T(8,128)(2,1)}) %reduce-scatter.8.cloned.1.call-update) | async-done | bytes 196624 | tf_op jit(solution)/shard_map/reduce_scatter | solution.py:133
  234.8 5.5 %all-to-all-start.2 = ((bf16[8,12,1024]{2,1,0:T(8,128)(2,1)}), bf16[8,12,1024]{2,1,0:T(8,128)(2,1)S(1)}, u32[]{:S(2)}, u32[]{:S(2)}) async-start(bf16[8,12,1024]{2,1,0:T(8,128)(2,1)} %reduce-scatter.8.cloned.1.call-done), calls=%async_computation.5 | async-start | bytes 524288 | tf_op jit(solution)/shard_map/all_to_all | solution.py:136
  240.3 0.1 copy.75
  240.6 9.1 %all-to-all-done.2 = bf16[8,12,1024]{2,1,0:T(8,128)(2,1)S(1)} async-done(((bf16[8,12,1024]{2,1,0:T(8,128)(2,1)}), bf16[8,12,1024]{2,1,0:T(8,128)(2,1)S(1)}, u32[]{:S(2)}, u32[]{:S(2)}) %all-to-all-start.2) | async-done | bytes 196640 | tf_op jit(solution)/shard_map/all_to_all | solution.py:136
  249.7 0.7 gather_fusion
  250.4 0.4 multiply_reduce_fusion.1
  250.8 49.3 %reduce-scatter.6.cloned.1.call-done = bf16[24,1024]{1,0:T(8,128)(2,1)} async-done(((bf16[192,1024]{1,0:T(8,128)(2,1)}), bf16[24,1024]{1,0:T(8,128)(2,1)}) %reduce-scatter.6.cloned.1.call-update) | async-done | bytes 49168 | tf_op jit(solution)/shard_map/reduce_scatter | solution.py:103
  300.1 1.6 add_convert_fusion
  (59 shorter events, 1.2 us)
Async XLA Ops:
  7.2 171.3 %copy-start = (bf16[1,256,4096]{2,1,0:T(8,128)(2,1)S(1)}, bf16[1,256,4096]{2,1,0:T(8,128)(2,1)}, u32[]{:S(2)}) copy-start(bf16[1,256,4096]{2,1,0:T(8,128)(2,1)} %param.39) | copy-start | bytes 6291460
  7.2 81.6 %reduce-scatter.4.cloned.1.call-start = ((), (), s32[]{:S(2)}) async-start(), calls=%async_computation.6 | async-start | bytes 663552 | tf_op jit(solution)/shard_map/reduce_scatter | solution.py:57
  9.5 17.8 %copy-start.10 = (f32[4]{0:T(128)S(1)}, f32[4]{0:T(128)}, u32[]{:S(2)}) copy-start(f32[4]{0:T(128)} %param.30) | copy-start | bytes 52
  9.5 20.0 %copy-start.5 = (s32[24,2]{0,1:T(2,128)S(1)}, s32[24,2]{0,1:T(2,128)}, u32[]{:S(2)}) copy-start(s32[24,2]{0,1:T(2,128)} %param.34) | copy-start | bytes 580
  89.8 8.2 %copy-start.1 = (f32[24,4,128,128]{3,2,1,0:T(8,128)S(1)}, f32[24,4,128,128]{3,2,1,0:T(8,128)}, u32[]{:S(2)}) copy-start(f32[24,4,128,128]{3,2,1,0:T(8,128)} %param.23) | copy-start | bytes 18874372
  102.1 7.6 %copy-start.8 = (f32[128]{0:T(128)S(1)}, f32[128]{0:T(128)}, u32[]{:S(2)}) copy-start(f32[128]{0:T(128)} %param.31) | copy-start | bytes 1540
  102.1 7.7 %copy-start.2 = (bf16[512,4096]{1,0:T(8,128)(2,1)S(1)}, bf16[512,4096]{1,0:T(8,128)(2,1)}, u32[]{:S(2)}) copy-start(bf16[512,4096]{1,0:T(8,128)(2,1)} %param.32) | copy-start | bytes 12582916
  109.9 9.4 %copy-start.3 = (bf16[24,4096]{1,0:T(8,128)(2,1)S(1)}, bf16[24,4096]{1,0:T(8,128)(2,1)}, u32[]{:S(2)}) copy-start(bf16[24,4096]{1,0:T(8,128)(2,1)} %param.22) | copy-start | bytes 589828
  109.9 10.4 %copy-start.4 = (f32[4096]{0:T(1024)S(1)}, f32[4096]{0:T(1024)}, u32[]{:S(2)}) copy-start(f32[4096]{0:T(1024)} %param.33) | copy-start | bytes 49156
  122.4 54.0 %all-to-all-start.1 = ((bf16[8,12,4096]{2,1,0:T(8,128)(2,1)}), bf16[8,12,4096]{2,1,0:T(8,128)(2,1)S(1)}, u32[]{:S(2)}, u32[]{:S(2)}) async-start(bf16[8,12,4096]{2,1,0:T(8,128)(2,1)} %reshape.153), calls=%async_computation.3 | async-start | bytes 2097152 | tf_op jit(solution)/shard_map/all_to_all | solution.py:124
  126.0 81.4 %all-reduce.2.cloned.1.call-start = ((), (), s32[]{:S(2)}) async-start(), calls=%async_computation.7 | async-start | bytes 786432 | tf_op jit(solution)/shard_map/psum | solution.py:99
  176.3 58.5 %reduce-scatter.8.cloned.1.call-start = ((), (), s32[]{:S(2)}) async-start(), calls=%async_computation.9 | async-start | bytes 1310720 | tf_op jit(solution)/shard_map/reduce_scatter | solution.py:133
  178.4 4.2 %copy-start.7 = (f32[24,2]{0,1:T(2,128)S(1)}, f32[24,2]{0,1:T(2,128)}, u32[]{:S(2)}) copy-start(f32[24,2]{0,1:T(2,128)} %param.36) | copy-start | bytes 580
  178.4 4.2 %copy-start.9 = (f32[24]{0:T(128)S(1)}, f32[24]{0:T(128)}, u32[]{:S(2)}) copy-start(f32[24]{0:T(128)} %param.35) | copy-start | bytes 292
  182.4 58.2 %copy-start.6 = (f32[1024]{0:T(1024)S(1)}, f32[1024]{0:T(1024)}, u32[]{:S(2)}) copy-start(f32[1024]{0:T(1024)} %param.43) | copy-start | bytes 12292
  182.4 117.7 %reduce-scatter.6.cloned.1.call-start = ((), (), s32[]{:S(2)}) async-start(), calls=%async_computation.8 | async-start | bytes 442368 | tf_op jit(solution)/shard_map/reduce_scatter | solution.py:103
  234.8 14.8 %all-to-all-start.2 = ((bf16[8,12,1024]{2,1,0:T(8,128)(2,1)}), bf16[8,12,1024]{2,1,0:T(8,128)(2,1)S(1)}, u32[]{:S(2)}, u32[]{:S(2)}) async-start(bf16[8,12,1024]{2,1,0:T(8,128)(2,1)} %reduce-scatter.8.cloned.1.call-done), calls=%async_computation.5 | async-start | bytes 524288 | tf_op jit(solution)/shard_map/all_to_all | solution.py:136
Sparse Core Ops, SparseCore 0:
  27.4 61.2 reduce-scatter.3
  176.4 30.9 all-reduce.1
  210.0 24.7 reduce-scatter.7
  238.0 62.1 reduce-scatter.5
